TPU v7x, 256 devices: a whole 4x4x8 slice. The times are simulated.
256 devices in a mesh: sp: 64 (over z, x, core), tp: 4 (over y).
Axes of the slice: x: 4, y: 4, z: 8, core: 2. Of those that a mesh axis runs over, the one named last changes fastest.
Arguments:
- queries: bfloat16 [8192, 2048], P('sp', 'tp'), may hold values from -6 to 6
- key_rows: bfloat16 [8192, 2048], P('sp', 'tp'), may hold values from -6 to 6
- value_rows: bfloat16 [8192, 2048], P('sp', 'tp'), may hold values from -6 to 6
- gate_input: bfloat16 [8192, 2048], P('sp', 'tp'), may hold values from -6 to 6
- log_decay: float32 [8192, 16], P('sp', 'tp'), may hold values from -0.6 to 0, as said below
- head_gain: float32 [2048], P('tp'), may hold values from 0.1 to 1.9
- out_weight: bfloat16 [2048, 2048], P('tp'), may hold values from -0.125 to 0.125
- residual: bfloat16 [8192, 2048], P('sp'), may hold values from -6 to 6
- mlp_gain: float32 [2048], replicated, may hold values from 0.1 to 1.9
- gate_weight: bfloat16 [2048, 5632], P('sp', 'tp'), may hold values from -0.125 to 0.125
- up_weight: bfloat16 [2048, 5632], P('sp', 'tp'), may hold values from -0.125 to 0.125
- down_weight: bfloat16 [5632, 2048], P('tp', 'sp'), may hold values from -0.078125 to 0.078125
Outputs:
- layer_out: bfloat16 [8192, 2048], P(('sp', 'tp'))
Inputs may be any that keep to these rules, and one draw needn't show every extreme that they name: log_decay holds the logarithm of a decay factor of each head at each position.
All inputs are finite; a program needn't handle non-finite values.
Results may differ from a plain program's by a relative error of at most 0.017.
Values may be sent and summed in bfloat16 or wider, within the bound.
A program may use at most 128 MiB of HBM per device.

v0:
```python
import jax
import jax.numpy as jnp
from jax import lax
from jax.sharding import Mesh
from jax.sharding import PartitionSpec as P

BLOCK = 128
SP = ("sp_0", "sp_1", "sp_2")
SP_TP = ("sp_0", "sp_1", "sp_2", "tp")
EPS = 1e-06


def gather_turned(arrays, axis, dims):
    turned = [jnp.moveaxis(a, dim, 0) for a, dim in zip(arrays, dims)]
    widths = [t[0].size for t in turned]
    both = jnp.concatenate([t.reshape(-1, w) for t, w in zip(turned, widths)], axis=1)
    filled = lax.all_gather(both, axis, axis=0, tiled=True)
    blocks = jnp.split(filled, [sum(widths[:k]) for k in range(1, len(widths))], axis=1)
    return tuple(
        (
            jnp.moveaxis(b.reshape(-1, *t.shape[1:]), 0, dim)
            for b, t, dim in zip(blocks, turned, dims)
        )
    )


def nothing_yet(x, identity):
    return jax.tree.map(
        lambda part, zero: jnp.zeros_like(part) + jnp.asarray(zero, part.dtype), x, identity
    )


def carried_in(x, axes, combine, identity):
    before = start = nothing_yet(x, identity)
    total = x
    for axis in reversed(axes):
        length, index = (lax.axis_size(axis), lax.axis_index(axis))
        pieces = jax.tree.map(
            lambda part, kind: lax.all_gather(part.astype(kind), axis),
            total,
            (jnp.bfloat16, jnp.bfloat16),
        )
        inside, total = (start, start)
        for k in range(length):
            passed = k < index
            total = combine(
                total, jax.tree.map(lambda part, own: part[k].astype(own.dtype), pieces, x)
            )
            inside = jax.tree.map(lambda new, old: jnp.where(passed, new, old), total, inside)
        before = combine(inside, before)
    return before


def copy_for_each(x, axis):
    length = lax.axis_size(axis)
    return lax.all_to_all(jnp.broadcast_to(x[None], (length, *x.shape)), axis, 0, 0, tiled=True)


def over_copies(x, axis):
    return copy_for_each(x, axis).astype(jnp.float32).sum(axis=0)


def split_up(x, dim, length):
    dims = x.shape
    blocks = x.reshape(*dims[:dim], length, dims[dim] // length, *dims[dim + 1 :])
    return jnp.moveaxis(blocks, dim, 0)


def sum_at_owner(x, axis, dim):
    blocks = split_up(x, dim, lax.axis_size(axis))
    arrived = lax.all_to_all(blocks, axis, split_axis=0, concat_axis=0, tiled=True)
    return arrived.astype(jnp.float32).sum(axis=0)


def rotate(values_in, positions):
    half = values_in.shape[-1] // 2
    freq = 10000.0 ** (-jnp.linspace(0.0, 1.0, half, dtype=jnp.float32))
    angles = positions * freq
    angles = jnp.concatenate([angles, angles], axis=-1)
    first = values_in[..., :half]
    second = values_in[..., half:]
    turned = jnp.concatenate([-second, first], axis=-1)
    return values_in * jnp.cos(angles) + turned * jnp.sin(angles)


def row_norm(stream, gain):
    return stream * lax.rsqrt(jnp.mean(stream * stream, axis=-1, keepdims=True) + EPS) * gain


def join_states(earlier, later):
    return (earlier[0] * later[0], later[0][:, None, None] * earlier[1] + later[1])


def body(
    queries,
    key_rows,
    value_rows,
    gate_input,
    log_decay,
    head_gain,
    out_weight,
    residual,
    mlp_gain,
    gate_weight,
    up_weight,
    down_weight,
):
    tok_rows = queries.shape[0]
    heads_here = log_decay.shape[1]
    head_size = head_gain.shape[0] // heads_here
    quarter = tok_rows // lax.axis_size("tp")
    full_gate, full_up, full_down = gather_turned(
        (gate_weight, up_weight, down_weight), SP, (0, 0, 1)
    )
    offset = lax.axis_index(SP) * tok_rows
    positions = (offset + lax.iota(jnp.int32, tok_rows)).astype(jnp.float32)[:, None, None]
    q_rot = rotate(
        queries.reshape(tok_rows, heads_here, head_size).astype(jnp.float32), positions
    ).astype(jnp.bfloat16)
    k_rot = (
        rotate(key_rows.reshape(tok_rows, heads_here, head_size).astype(jnp.float32), positions)
        * head_size ** (-0.5)
    ).astype(jnp.bfloat16)
    blocks = tok_rows // BLOCK
    q_blocks = q_rot.reshape(blocks, BLOCK, heads_here, head_size)
    k_blocks = k_rot.reshape(blocks, BLOCK, heads_here, head_size)
    v_blocks = value_rows.reshape(blocks, BLOCK, heads_here, head_size)
    cumul = jnp.cumsum(log_decay.reshape(blocks, BLOCK, heads_here), axis=1)
    by_head = cumul.transpose(0, 2, 1)
    lower = jnp.tril(jnp.ones((BLOCK, BLOCK), dtype=bool))
    spread = by_head[:, :, :, None] - by_head[:, :, None, :]
    weight = jnp.where(lower, jnp.exp(jnp.where(lower, spread, 0.0)), 0.0)
    scores = jnp.einsum("nthd,nshd->nhts", q_blocks, k_blocks, preferred_element_type=jnp.float32)
    probs = (scores * weight).astype(jnp.bfloat16)
    inner = jnp.einsum("nhts,nshe->nthe", probs, v_blocks, preferred_element_type=jnp.float32)
    k_weighted = (
        k_blocks.astype(jnp.float32) * jnp.exp(cumul[:, -1:, :] - cumul)[..., None]
    ).astype(jnp.bfloat16)
    contrib = jnp.einsum(
        "nshd,nshe->nhde", k_weighted, v_blocks, preferred_element_type=jnp.float32
    )
    totals = jnp.exp(cumul[:, -1, :])

    def advance(carry, items):
        state, prefix = carry
        factor, update = items
        return ((state * factor[:, None, None] + update, prefix * factor), (state, prefix))

    start_state = jnp.zeros((heads_here, head_size, head_size), jnp.float32)
    start_prefix = jnp.ones((heads_here,), jnp.float32)
    (dev_state, dev_total), (local_before, prefixes) = lax.scan(
        advance, (start_state, start_prefix), (totals, contrib)
    )
    _, incoming = carried_in((dev_total, dev_state), SP, join_states, (start_prefix, start_state))
    before = local_before + prefixes[:, :, None, None] * incoming[None]
    cross = jnp.einsum(
        "nthd,nhde->nthe", q_blocks.astype(jnp.float32), before, precision=lax.Precision.HIGHEST
    )
    cross = cross * jnp.exp(cumul)[..., None]
    result = (inner + cross).reshape(tok_rows, heads_here, head_size)
    result = row_norm(result, head_gain.reshape(heads_here, head_size)).reshape(
        tok_rows, heads_here * head_size
    )
    retained = (result * jax.nn.silu(gate_input.astype(jnp.float32))).astype(jnp.bfloat16)
    partial_value = jnp.dot(retained, out_weight, preferred_element_type=jnp.float32)
    mixed = over_copies(partial_value.astype(jnp.bfloat16), "tp").astype(jnp.float32)
    middle = (residual.astype(jnp.float32) + mixed).astype(jnp.bfloat16)
    normed = row_norm(middle.astype(jnp.float32), mlp_gain).astype(jnp.bfloat16)
    rows_mid = lax.dynamic_slice_in_dim(middle, lax.axis_index("tp") * quarter, quarter, 0)
    gate = jnp.dot(normed, full_gate, preferred_element_type=jnp.float32)
    upvals = jnp.dot(normed, full_up, preferred_element_type=jnp.float32)
    hidden = (jax.nn.silu(gate) * upvals).astype(jnp.bfloat16)
    ffn = sum_at_owner(
        jnp.dot(hidden, full_down, preferred_element_type=jnp.float32).astype(jnp.bfloat16), "tp", 0
    )
    return (rows_mid.astype(jnp.float32) + ffn).astype(jnp.bfloat16)


def solution(mesh):
    finer = Mesh(mesh.devices.reshape(8, 4, 2, mesh.shape["tp"]), ("sp_0", "sp_1", "sp_2", "tp"))
    in_specs = (
        P(SP, "tp"),
        P(SP, "tp"),
        P(SP, "tp"),
        P(SP, "tp"),
        P(SP, "tp"),
        P("tp"),
        P("tp", None),
        P(SP, None),
        P(),
        P(SP, "tp"),
        P(SP, "tp"),
        P("tp", SP),
    )
    out_specs = P(SP_TP, None)
    return jax.shard_map(body, mesh=finer, in_specs=in_specs, out_specs=out_specs, check_vma=False)
```

profile of v0, /device:TPU:1, one launch (start us, length us, event | category | flops | bytes accessed | tf_op | source)
XLA Modules:
  0.0 215.4 jit_solution(10362698421659114462)
XLA Ops:
  6.6 0.9 copy.69
  7.5 0.2 reduce_window_sum.13
  7.8 4.7 %all-gather = bf16[2,1,4]{2,1,0:T(2,128)(2,1)S(1)} all-gather(bf16[1,1,4]{2,1,0:T(2,128)(2,1)S(1)} %get-tuple-element.38), channel_id=2, replica_groups=mesh['sp_0'=8,'sp_1'=4,'sp_2'=2,'tp'=4] {'sp_2'}, dimensions={0}, use_global_device_ids=true | all-gather | bytes 24 | tf_op jit(solution)/shard_map/all_gather | solution.py:39
  12.7 0.3 fusion.150
  13.0 0.9 copy_bitcast_fusion
  13.9 0.9 copy_bitcast_fusion.1
  14.8 0.2 slice_negate_fusion
  15.1 1.2 fusion.39
  16.3 1.2 fusion.20
  17.6 2.0 all-gather.1
  19.6 6.0 %all-gather.2 = bf16[4,1,4]{2,1,0:T(2,128)(2,1)S(1)} all-gather(bf16[1,1,4]{2,1,0:T(2,128)(2,1)S(1)} %multiply_convert_fusion.2), channel_id=1, replica_groups=mesh['sp_0'=8,'sp_1'=4,'sp_2'=2,'tp'=4] {'sp_1'}, dimensions={0}, use_global_device_ids=true | all-gather | bytes 40 | tf_op jit(solution)/shard_map/all_gather | solution.py:39
  25.6 0.1 fusion.90
  25.7 11.4 %all_gather.31 = bf16[4,4,128,128]{3,2,1,0:T(8,128)(2,1)S(1)} all-gather(bf16[1,4,128,128]{3,2,1,0:T(8,128)(2,1)S(1)} %fusion.90), channel_id=1, replica_groups=mesh['sp_0'=8,'sp_1'=4,'sp_2'=2,'tp'=4] {'sp_1'}, dimensions={0}, use_global_device_ids=true | all-gather | bytes 655360 | tf_op jit(solution)/shard_map/all_gather | solution.py:39
  37.0 0.8 fusion.84
  38.0 0.7 pad_maximum_fusion
  38.7 14.3 %all-gather.3 = bf16[8,1,4]{2,1,0:T(2,128)(2,1)S(1)} all-gather(bf16[1,1,4]{2,1,0:T(2,128)(2,1)S(1)} %fusion.164), channel_id=1, replica_groups=mesh['sp_0'=8,'sp_1'=4,'sp_2'=2,'tp'=4] {'sp_0'}, dimensions={0}, use_global_device_ids=true | all-gather | bytes 72 | tf_op jit(solution)/shard_map/all_gather | solution.py:39
  53.1 2.0 convolution_bitcast_fusion.1
  55.1 20.8 %all-gather.7.cloned.1.call-done = bf16[8,4,128,128]{3,2,1,0:T(8,128)(2,1)} async-done(((bf16[1,4,128,128]{3,2,1,0:T(8,128)(2,1)}), bf16[8,4,128,128]{3,2,1,0:T(8,128)(2,1)}) %all-gather.7.cloned.1.call-update) | async-done | bytes 1048592 | tf_op jit(solution)/shard_map/all_gather | solution.py:39
  76.0 2.3 %multiply_reduce_fusion = (f32[128,4]{0,1:T(4,128)S(1)}, f32[1,128,4,128]{1,3,2,0:T(8,128)S(1)}) fusion(f32[1,128,4,128]{1,3,2,0:T(8,128)} %convolution_bitcast_fusion.1, f32[128,4]{0,1:T(4,128)S(1)} %get-tuple-element.49, bf16[128,4,128]{2,0,1:T(8,128)(2,1)S(1)} %get-tuple-element.36, bf16[8,4,128,128]{3,2,1,0:T(8,128)(2,1)} %all-gather.7.cloned.1.call-done, ...), kind=kOutput, calls=%fused_computation.63 | convolution fusion | flops 104660480 | bytes 2494734 | tf_op jit(solution)/shard_map/nthd,nhde->nthe/dot_general | solution.py:156
  78.4 0.1 copy.78
  78.6 0.2 mul.480
  78.8 0.5 convolution_convert_fusion
  79.3 0.2 broadcast_in_dim.36
  79.6 24.2 %all_to_all.10 = bf16[4,128,2048]{2,1,0:T(8,128)(2,1)S(1)} all-to-all(bf16[4,128,2048]{2,1,0:T(8,128)(2,1)S(1)} %broadcast_in_dim.36), channel_id=1, replica_groups=mesh['sp_0'=8,'sp_1'=4,'sp_2'=2,'tp'=4] {'tp'}, dimensions={0} | all-to-all | bytes 4194304 | tf_op jit(solution)/shard_map/all_to_all | solution.py:56
  103.8 0.4 convert_reduce_fusion
  104.2 0.2 fusion.21
  104.4 78.6 %all-gather.9.cloned.1.call-done = bf16[2048,4224]{1,0:T(8,128)(2,1)} async-done(((bf16[32,4224]{1,0:T(8,128)(2,1)}), bf16[2048,4224]{1,0:T(8,128)(2,1)}) %all-gather.9.cloned.1.call-update) | async-done | bytes 17301520 | tf_op jit(solution)/shard_map/all_gather | solution.py:17
  183.0 3.7 %fusion.4 = f32[128,1408]{1,0:T(8,128)S(1)} fusion(bf16[2048,4224]{1,0:T(8,128)(2,1)} %all-gather.9.cloned.1.call-done, bf16[128,2048]{1,0:T(8,128)(2,1)S(1)} %get-tuple-element.19, f32[2048]{0:T(1024)S(1)} %copy-done.6, f32[128]{0:T(128)S(1)} %add_rsqrt_fusion.1), kind=kOutput, calls=%fused_computation.4 | convolution fusion | flops 739246080 | bytes 7021056 | tf_op jit(solution)/shard_map/dot_general | solution.py:170
  186.7 8.0 %fusion.9 = bf16[128,2048]{1,0:T(8,128)(2,1)} fusion(bf16[2048,4224]{1,0:T(8,128)(2,1)} %all-gather.9.cloned.1.call-done, f32[128,1408]{1,0:T(8,128)S(1)} %fusion.4, bf16[128,2048]{1,0:T(8,128)(2,1)S(1)} %get-tuple-element.19, f32[2048]{0:T(1024)S(1)} %copy-done.6, f32[128]{0:T(128)S(1)} %add_rsqrt_fusion.1), kind=kOutput, calls=%fused_computation.8 | convolution fusion | flops 1478787072 | bytes 13312512 | tf_op jit(solution)/shard_map/dot_general | solution.py:174
  194.7 4.0 %all-to-all-start.1 = ((bf16[4,32,2048]{2,1,0:T(8,128)(2,1)}), bf16[4,32,2048]{2,1,0:T(8,128)(2,1)S(1)}, u32[]{:S(2)}, u32[]{:S(2)}) async-start(bf16[4,32,2048]{2,1,0:T(8,128)(2,1)} %bitcast.176), calls=%async_computation.1 | async-start | bytes 1048576 | tf_op jit(solution)/shard_map/all_to_all | solution.py:71
  198.7 9.0 %all-to-all-done.1 = bf16[4,32,2048]{2,1,0:T(8,128)(2,1)S(1)} async-done(((bf16[4,32,2048]{2,1,0:T(8,128)(2,1)}), bf16[4,32,2048]{2,1,0:T(8,128)(2,1)S(1)}, u32[]{:S(2)}, u32[]{:S(2)}) %all-to-all-start.1) | async-done | bytes 524320 | tf_op jit(solution)/shard_map/all_to_all | solution.py:71
  207.8 0.7 add_convert_fusion.1
  (41 shorter events, 0.8 us)
Async XLA Ops:
  6.5 72.2 %copy-start = (bf16[512,2048]{1,0:T(8,128)(2,1)S(1)}, bf16[512,2048]{1,0:T(8,128)(2,1)}, u32[]{:S(2)}) copy-start(bf16[512,2048]{1,0:T(8,128)(2,1)} %param.20) | copy-start | bytes 6291460
  6.5 31.4 %copy-start.2 = (bf16[1408,32]{0,1:T(8,128)(2,1)S(1)}, bf16[1408,32]{0,1:T(8,128)(2,1)}, u32[]{:S(2)}) copy-start(bf16[1408,32]{0,1:T(8,128)(2,1)} %param.25) | copy-start | bytes 270340
  6.5 31.4 %copy-start.4 = (bf16[32,1408]{1,0:T(8,128)(2,1)S(1)}, bf16[32,1408]{1,0:T(8,128)(2,1)}, u32[]{:S(2)}) copy-start(bf16[32,1408]{1,0:T(8,128)(2,1)} %param.23) | copy-start | bytes 270340
  6.5 31.4 %copy-start.3 = (bf16[32,1408]{1,0:T(8,128)(2,1)S(1)}, bf16[32,1408]{1,0:T(8,128)(2,1)}, u32[]{:S(2)}) copy-start(bf16[32,1408]{1,0:T(8,128)(2,1)} %param.24) | copy-start | bytes 270340
  6.5 69.4 %all-gather.7.cloned.1.call-start = ((), (), s32[]{:S(2)}) async-start(), calls=%async_computation.2 | async-start | bytes 1179648 | tf_op jit(solution)/shard_map/all_gather | solution.py:39
  15.1 63.7 %copy-start.7 = (f32[512]{0:T(512)S(1)}, f32[512]{0:T(512)}, u32[]{:S(2)}) copy-start(f32[512]{0:T(512)} %param.19) | copy-start | bytes 6148
  37.9 145.1 %all-gather.9.cloned.1.call-start = ((), (), s32[]{:S(2)}) async-start(), calls=%async_computation.3 | async-start | bytes 17571840 | tf_op jit(solution)/shard_map/all_gather | solution.py:17
  55.1 23.7 %copy-start.5 = (bf16[128,512]{1,0:T(8,128)(2,1)S(1)}, bf16[128,512]{1,0:T(8,128)(2,1)}, u32[]{:S(2)}) copy-start(bf16[128,512]{1,0:T(8,128)(2,1)} %param.17) | copy-start | bytes 393220
  79.3 24.9 %copy-start.1 = (bf16[128,2048]{1,0:T(8,128)(2,1)S(1)}, bf16[128,2048]{1,0:T(8,128)(2,1)}, u32[]{:S(2)}) copy-start(bf16[128,2048]{1,0:T(8,128)(2,1)} %param.21) | copy-start | bytes 1572868
  79.3 103.7 %copy-start.6 = (f32[2048]{0:T(1024)S(1)}, f32[2048]{0:T(1024)}, u32[]{:S(2)}) copy-start(f32[2048]{0:T(1024)} %param.22) | copy-start | bytes 24580
  194.7 13.0 %all-to-all-start.1 = ((bf16[4,32,2048]{2,1,0:T(8,128)(2,1)}), bf16[4,32,2048]{2,1,0:T(8,128)(2,1)S(1)}, u32[]{:S(2)}, u32[]{:S(2)}) async-start(bf16[4,32,2048]{2,1,0:T(8,128)(2,1)} %bitcast.176), calls=%async_computation.1 | async-start | bytes 1048576 | tf_op jit(solution)/shard_map/all_to_all | solution.py:71
Sparse Core Ops, SparseCore 0:
  38.0 37.9 all-gather.6
  78.7 104.2 all-gather.8
where the time goes:
time: 216 us; the launch traced here: 215 us
  waiting for transfers between devices  108 us (50%)
  blocking collectives  62.5 us (29%)
  matrix products  17.7 us (8%)
  between operations  13.6 us (6%)
  other arithmetic  7.15 us (3%)
  starting transfers between devices  4.07 us (2%)
    all_gather x1, waiting for transfers between devices, gather_turned(): filled = lax.all_gather(both, axis, axis=0, tiled=True)  78.6 us
    all_gather x5, blocking collectives, carried_in(): lax.all_gather(part.astype(kind), axis)  38.3 us
    all_to_all x1, blocking collectives, copy_for_each(): lax.all_to_all(jnp.broadcast_to(x[None], (length, *x.shape)), axis, 0, 0,...  24.2 us
    all_gather x1, waiting for transfers between devices, carried_in(): lax.all_gather(part.astype(kind), axis)  20.8 us
    all_to_all x1, waiting for transfers between devices, sum_at_owner(): lax.all_to_all(blocks, axis, split_axis=0, concat_axis=0, tiled=True)  9.03 us
    dot_general x1, matrix products, body(): jnp.dot(hidden, full_down, preferred_element_type=jnp.float32)  8.02 us
  transfers between devices with their start and end apart: 3, of which 3 were waited for; matrix products, arithmetic and copies ran while one was open for 3% of the time, Pallas kernels for 0%

commit v1 on v0

--- a/solution.py
+++ b/solution.py
@@ -10,11 +10,18 @@
 EPS = 1e-06
 
 
+def targets_process(vals, across):
+    sheets = []
+    for _ in range(lax.axis_size(across)):
+        sheets.append(vals)
+    return jnp.concatenate(lax.all_to_all(jnp.stack(sheets, axis=0), across, 0, 0), axis=0)
+
+
 def gather_turned(arrays, axis, dims):
     turned = [jnp.moveaxis(a, dim, 0) for a, dim in zip(arrays, dims)]
     widths = [t[0].size for t in turned]
     both = jnp.concatenate([t.reshape(-1, w) for t, w in zip(turned, widths)], axis=1)
-    filled = lax.all_gather(both, axis, axis=0, tiled=True)
+    filled = targets_process(both, axis)
     blocks = jnp.split(filled, [sum(widths[:k]) for k in range(1, len(widths))], axis=1)
     return tuple(
         (

time: 216 us -> 545 us (2.52); the launches traced: 215 us -> 536 us
  waiting for transfers between devices: 108 us -> 424 us
  blocking collectives: 62.5 us -> 39.9 us
  starting transfers between devices: 4.07 us -> 22.8 us
  local copies, waits for them, and re-layouts: 1.78 us -> 9.27 us
    all_to_all x0 -> x2, waiting for transfers between devices: none -> 395 us  [the longest x1 374 us: targets_process(): lax.all_to_all(jnp.stack(sheets, axis=0), across, 0, 0)]
    all_gather x1 -> x0, waiting for transfers between devices: 78.6 us -> none  [gather_turned(): filled = lax.all_gather(both, axis, axis=0, tiled=True)]
    all_to_all x1 -> x0, blocking collectives: 24.2 us -> none  [copy_for_each(): lax.all_to_all(jnp.broadcast_to(x[None], (length, *x.shape)), axis, 0, 0,...]
    all_to_all x0 -> x2, starting transfers between devices: none -> 19.3 us  [the longest x1 14.9 us: targets_process(): lax.all_to_all(jnp.stack(sheets, axis=0), across, 0, 0)]
    another operation x0 -> x1, local copies, waits for them, and re-layouts: none -> 6.1 us  [targets_process(): jnp.stack(sheets, axis=0)]
  transfers between devices with their start and end apart: 3 -> 4, of which waited for: 3 -> 4; matrix products, arithmetic and copies ran while one was open for 3% -> 1% of each run, Pallas kernels for 0% -> 0%
where the time goes in v1:
time: 545 us; the launch traced here: 536 us
  waiting for transfers between devices  424 us (78%)
  blocking collectives  39.9 us (7%)
  starting transfers between devices  22.8 us (4%)
  matrix products  17.9 us (3%)
  between operations  13.7 us (3%)
  local copies, waits for them, and re-layouts  9.27 us (2%)
  other arithmetic  8.17 us (1%)
    all_to_all x1, waiting for transfers between devices, targets_process(): lax.all_to_all(jnp.stack(sheets, axis=0), across, 0, 0)  374 us
    all_gather x5, blocking collectives, carried_in(): lax.all_gather(part.astype(kind), axis)  39.9 us
    all_gather x1, waiting for transfers between devices, carried_in(): lax.all_gather(part.astype(kind), axis)  21.5 us
    all_to_all x1, waiting for transfers between devices, copy_for_each(): lax.all_to_all(jnp.broadcast_to(x[None], (length, *x.shape)), axis, 0, 0,...  20.4 us
    all_to_all x1, starting transfers between devices, targets_process(): lax.all_to_all(jnp.stack(sheets, axis=0), across, 0, 0)  14.9 us
  transfers between devices with their start and end apart: 4, of which 4 were waited for; matrix products, arithmetic and copies ran while one was open for 1% of the time, Pallas kernels for 0%

profile of v1, /device:TPU:1, one launch (start us, length us, event | category | flops | bytes accessed | tf_op | source)
XLA Modules:
  0.0 535.6 jit_solution(16057579667690061415)
XLA Ops:
  6.6 1.0 copy.69
  7.5 0.2 reduce_window_sum.13
  7.8 4.7 all-gather
  12.5 0.9 copy_bitcast_fusion
  13.4 0.9 copy_bitcast_fusion.1
  14.5 0.3 fusion.150
  14.8 6.0 %all-gather.2 = bf16[4,1,4]{2,1,0:T(2,128)(2,1)S(1)} all-gather(bf16[1,1,4]{2,1,0:T(2,128)(2,1)S(1)} %multiply_convert_fusion.2), channel_id=1, replica_groups=mesh['sp_0'=8,'sp_1'=4,'sp_2'=2,'tp'=4] {'sp_1'}, dimensions={0}, use_global_device_ids=true | all-gather | bytes 40 | tf_op jit(solution)/shard_map/all_gather | solution.py:46
  20.8 0.2 slice_negate_fusion
  21.1 1.2 fusion.39
  22.3 1.2 fusion.20
  23.6 4.0 all-gather.1
  27.7 9.9 %all_gather.28 = bf16[4,4,128,128]{3,2,1,0:T(8,128)(2,1)S(1)} all-gather(bf16[1,4,128,128]{3,2,1,0:T(8,128)(2,1)S(1)} %fusion.90), channel_id=1, replica_groups=mesh['sp_0'=8,'sp_1'=4,'sp_2'=2,'tp'=4] {'sp_1'}, dimensions={0}, use_global_device_ids=true | all-gather | bytes 655360 | tf_op jit(solution)/shard_map/all_gather | solution.py:46
  37.6 0.8 fusion.84
  38.5 15.4 %all-gather.3 = bf16[8,1,4]{2,1,0:T(2,128)(2,1)S(1)} all-gather(bf16[1,1,4]{2,1,0:T(2,128)(2,1)S(1)} %fusion.164), channel_id=1, replica_groups=mesh['sp_0'=8,'sp_1'=4,'sp_2'=2,'tp'=4] {'sp_0'}, dimensions={0}, use_global_device_ids=true | all-gather | bytes 72 | tf_op jit(solution)/shard_map/all_gather | solution.py:46
  54.0 1.1 convolution_bitcast_fusion.1
  55.1 21.5 %all-gather.6.cloned.1.call-done = bf16[8,4,128,128]{3,2,1,0:T(8,128)(2,1)} async-done(((bf16[1,4,128,128]{3,2,1,0:T(8,128)(2,1)}), bf16[8,4,128,128]{3,2,1,0:T(8,128)(2,1)}) %all-gather.6.cloned.1.call-update) | async-done | bytes 1048592 | tf_op jit(solution)/shard_map/all_gather | solution.py:46
  76.6 2.4 multiply_reduce_fusion
  79.3 0.2 mul.480
  79.5 0.5 convolution_convert_fusion
  80.0 1.6 broadcast_in_dim.36
  81.6 4.5 all-to-all-start
  86.1 20.4 %all-to-all-done = bf16[4,128,2048]{2,1,0:T(8,128)(2,1)} async-done(((bf16[4,128,2048]{2,1,0:T(8,128)(2,1)}), bf16[4,128,2048]{2,1,0:T(8,128)(2,1)}, u32[]{:S(2)}, u32[]{:S(2)}) %all-to-all-start) | async-done | bytes 2097184 | tf_op jit(solution)/shard_map/all_to_all | solution.py:63
  106.5 6.1 %stack.2 = bf16[64,32,4224]{2,1,0:T(8,128)(2,1)} broadcast(bf16[32,4224]{1,0:T(8,128)(2,1)S(1)} %pad_maximum_fusion), dimensions={1,2} | broadcast | bytes 17571840 | tf_op jit(solution)/shard_map/stack | solution.py:17
  112.6 14.9 %all-to-all-start.1 = ((bf16[64,32,4224]{2,1,0:T(8,128)(2,1)}), bf16[64,32,4224]{2,1,0:T(8,128)(2,1)}, u32[]{:S(2)}, u32[]{:S(2)}) async-start(bf16[64,32,4224]{2,1,0:T(8,128)(2,1)} %stack.2), calls=%async_computation.1 | async-start | bytes 34603008 | tf_op jit(solution)/shard_map/all_to_all | solution.py:17
  127.5 2.1 convert_reduce_fusion
  129.6 0.3 fusion.21
  129.9 374.1 %all-to-all-done.1 = bf16[64,32,4224]{2,1,0:T(8,128)(2,1)} async-done(((bf16[64,32,4224]{2,1,0:T(8,128)(2,1)}), bf16[64,32,4224]{2,1,0:T(8,128)(2,1)}, u32[]{:S(2)}, u32[]{:S(2)}) %all-to-all-start.1) | async-done | bytes 17301536 | tf_op jit(solution)/shard_map/all_to_all | solution.py:17
  504.0 4.5 fusion.4
  508.5 8.2 %fusion.9 = bf16[128,2048]{1,0:T(8,128)(2,1)} fusion(bf16[2048,4224]{1,0:T(8,128)(2,1)} %bitcast.34, f32[128,1408]{1,0:T(8,128)} %fusion.4, bf16[128,2048]{1,0:T(8,128)(2,1)S(1)} %get-tuple-element.19, f32[2048]{0:T(1024)S(1)} %copy-done.7, f32[128]{0:T(128)S(1)} %add_rsqrt_fusion.1), kind=kOutput, calls=%fused_computation.8 | convolution fusion | flops 1478787072 | bytes 13312512 | tf_op jit(solution)/shard_map/dot_general | solution.py:181
  516.7 3.5 all-to-all-start.2
  520.2 7.8 %all-to-all-done.2 = bf16[4,32,2048]{2,1,0:T(8,128)(2,1)S(1)} async-done(((bf16[4,32,2048]{2,1,0:T(8,128)(2,1)}), bf16[4,32,2048]{2,1,0:T(8,128)(2,1)S(1)}, u32[]{:S(2)}, u32[]{:S(2)}) %all-to-all-start.2) | async-done | bytes 524320 | tf_op jit(solution)/shard_map/all_to_all | solution.py:78
  528.1 0.7 add_convert_fusion.1
  (44 shorter events, 1.0 us)
Async XLA Ops:
  6.5 72.9 %copy-start = (bf16[512,2048]{1,0:T(8,128)(2,1)S(1)}, bf16[512,2048]{1,0:T(8,128)(2,1)}, u32[]{:S(2)}) copy-start(bf16[512,2048]{1,0:T(8,128)(2,1)} %param.20) | copy-start | bytes 6291460
  6.5 47.4 %copy-start.5 = (bf16[128,512]{1,0:T(8,128)(2,1)S(1)}, bf16[128,512]{1,0:T(8,128)(2,1)}, u32[]{:S(2)}) copy-start(bf16[128,512]{1,0:T(8,128)(2,1)} %param.16) | copy-start | bytes 393220
  6.5 70.1 %all-gather.6.cloned.1.call-start = ((), (), s32[]{:S(2)}) async-start(), calls=%async_computation.3 | async-start | bytes 1179648 | tf_op jit(solution)/shard_map/all_gather | solution.py:46
  21.1 58.4 %copy-start.6 = (bf16[128,512]{1,0:T(8,128)(2,1)S(1)}, bf16[128,512]{1,0:T(8,128)(2,1)}, u32[]{:S(2)}) copy-start(bf16[128,512]{1,0:T(8,128)(2,1)} %param.17) | copy-start | bytes 393220
  21.1 58.4 %copy-start.8 = (f32[512]{0:T(512)S(1)}, f32[512]{0:T(512)}, u32[]{:S(2)}) copy-start(f32[512]{0:T(512)} %param.19) | copy-start | bytes 6148
  79.0 7.1 %copy-start.2 = (bf16[1408,32]{0,1:T(8,128)(2,1)S(1)}, bf16[1408,32]{0,1:T(8,128)(2,1)}, u32[]{:S(2)}) copy-start(bf16[1408,32]{0,1:T(8,128)(2,1)} %param.25) | copy-start | bytes 270340
  79.0 7.1 %copy-start.3 = (bf16[32,1408]{1,0:T(8,128)(2,1)S(1)}, bf16[32,1408]{1,0:T(8,128)(2,1)}, u32[]{:S(2)}) copy-start(bf16[32,1408]{1,0:T(8,128)(2,1)} %param.24) | copy-start | bytes 270340
  79.0 7.1 %copy-start.4 = (bf16[32,1408]{1,0:T(8,128)(2,1)S(1)}, bf16[32,1408]{1,0:T(8,128)(2,1)}, u32[]{:S(2)}) copy-start(bf16[32,1408]{1,0:T(8,128)(2,1)} %param.23) | copy-start | bytes 270340
  81.6 25.0 %all-to-all-start = ((bf16[4,128,2048]{2,1,0:T(8,128)(2,1)}), bf16[4,128,2048]{2,1,0:T(8,128)(2,1)}, u32[]{:S(2)}, u32[]{:S(2)}) async-start(bf16[4,128,2048]{2,1,0:T(8,128)(2,1)} %broadcast_in_dim.36), calls=%async_computation | async-start | bytes 4194304 | tf_op jit(solution)/shard_map/all_to_all | solution.py:63
  112.6 17.0 %copy-start.1 = (bf16[128,2048]{1,0:T(8,128)(2,1)S(1)}, bf16[128,2048]{1,0:T(8,128)(2,1)}, u32[]{:S(2)}) copy-start(bf16[128,2048]{1,0:T(8,128)(2,1)} %param.21) | copy-start | bytes 1572868
  112.6 391.3 %copy-start.7 = (f32[2048]{0:T(1024)S(1)}, f32[2048]{0:T(1024)}, u32[]{:S(2)}) copy-start(f32[2048]{0:T(1024)} %param.22) | copy-start | bytes 24580
  112.6 391.3 %all-to-all-start.1 = ((bf16[64,32,4224]{2,1,0:T(8,128)(2,1)}), bf16[64,32,4224]{2,1,0:T(8,128)(2,1)}, u32[]{:S(2)}, u32[]{:S(2)}) async-start(bf16[64,32,4224]{2,1,0:T(8,128)(2,1)} %stack.2), calls=%async_computation.1 | async-start | bytes 34603008 | tf_op jit(solution)/shard_map/all_to_all | solution.py:17
  516.7 11.3 %all-to-all-start.2 = ((bf16[4,32,2048]{2,1,0:T(8,128)(2,1)}), bf16[4,32,2048]{2,1,0:T(8,128)(2,1)S(1)}, u32[]{:S(2)}, u32[]{:S(2)}) async-start(bf16[4,32,2048]{2,1,0:T(8,128)(2,1)} %bitcast.177), calls=%async_computation.2 | async-start | bytes 1048576 | tf_op jit(solution)/shard_map/all_to_all | solution.py:78
Sparse Core Ops, SparseCore 0:
  38.6 37.9 all-gather.5
